TPU v7x, 32 devices: a whole 2x2x4 slice. The times are simulated.
32 devices in a mesh: grp: 2 (over y), sp: 4 (over z), tp: 4 (over x, core).
Axes of the slice: x: 2, y: 2, z: 4, core: 2. Of those that a mesh axis runs over, the one named last changes fastest.
Arguments:
- conv_input: bfloat16 [4096, 1024], P(('grp', 'sp'), 'tp'), parts along dimension 0, may hold values from -6 to 6
- pre_gate: bfloat16 [4096, 1024], P(('grp', 'sp'), 'tp'), parts along dimension 0, may hold values from -6 to 6
- post_gate: bfloat16 [4096, 1024], P(('grp', 'sp'), 'tp'), parts along dimension 0, may hold values from -6 to 6
- conv_taps: float32 [3, 1024], replicated, may hold values from -3.5 to 3.5
- out_proj: bfloat16 [1024, 2048], replicated, may hold values from -0.1875 to 0.1875
- residual_in: bfloat16 [4096, 2048], P(('grp', 'sp', 'tp')), parts along dimension 0, may hold values from -6 to 6
- norm_gain: float32 [2048], replicated, may hold values from 0.1 to 1.9
- routes: int32 [4096, 2], P(('grp', 'sp', 'tp')), parts along dimension 0, may hold values from 0 to 7, as said below
- route_weight: float32 [4096, 2], P(('grp', 'sp', 'tp')), parts along dimension 0, may hold values from 0.1 to 1
- w_gate: bfloat16 [8, 2048, 1024], P('sp', None, 'tp'), may hold values from -0.125 to 0.125
- w_up: bfloat16 [8, 2048, 1024], P('sp', None, 'tp'), may hold values from -0.125 to 0.125
- w_down: bfloat16 [8, 1024, 2048], P('sp', 'tp'), may hold values from -0.1875 to 0.1875
Outputs:
- layer_out: bfloat16 [4096, 2048], P(('grp', 'sp', 'tp')), parts along dimension 0
There are 2 independent parts, one for each index of `grp`. A program takes and returns all parts, laid end to end along the dimension named above; an argument that names none is the same for every part. Nothing has to cross between parts.
Inputs may be any that keep to these rules, and one draw needn't show every extreme that they name: `routes`: the two numbers of a row differ and lie in the same group of 2 consecutive experts. In each aligned block of 128 rows every expert is named exactly 32 times.
All inputs are finite; a program needn't handle non-finite values.
Results may differ from a plain program's by a relative error of at most 0.0085.
Values may be sent and summed in bfloat16 or wider, within the bound.
No kernel may reach another device: no remote copies, remote signals or barrier semaphores. Data moves between devices by JAX's collectives and lax.ppermute only.
A program may use at most 64 MiB of HBM per device.

v0:
```python
import jax
import jax.numpy as jnp
from jax import lax
from jax.sharding import PartitionSpec as P

GROUPS = 4
LANES = 128


def shifted(block, axis, distance):
    devices = range(lax.axis_size(axis))
    route = [(i - distance, i) for i in devices if i - distance in devices]
    return lax.ppermute(block, axis, route)


def flipped(block, axis, bit):
    return lax.ppermute(block, axis, [(i, i ^ bit) for i in range(lax.axis_size(axis))])


def mix(conv_input, pre_gate, post_gate, conv_taps):
    channels = conv_input.shape[1]
    taps = lax.dynamic_slice_in_dim(conv_taps, lax.axis_index("tp") * channels, channels, 1)
    edge = jnp.concatenate([conv_input[-2:], pre_gate[-2:]], axis=1)
    prior = shifted(edge, "sp", 1)
    prior_input, prior_gate = (prior[:, :channels], prior[:, channels:])
    gated = jnp.concatenate(
        [
            prior_gate.astype(jnp.float32) * prior_input.astype(jnp.float32),
            pre_gate.astype(jnp.float32) * conv_input.astype(jnp.float32),
        ],
        axis=0,
    )
    conv = gated[2:] * taps[2] + gated[1:-1] * taps[1] + gated[:-2] * taps[0]
    return (post_gate.astype(jnp.float32) * conv).astype(jnp.bfloat16)


def project(mixed, out_proj, residual_in, norm_gain):
    token_rows = lax.all_to_all(mixed, "tp", split_axis=0, concat_axis=1, tiled=True)
    projected = jnp.dot(token_rows, out_proj, preferred_element_type=jnp.float32)
    stream = residual_in.astype(jnp.float32) + projected
    scale = lax.rsqrt(jnp.mean(stream * stream, axis=-1, keepdims=True) + 1e-06)
    normed = (stream * scale * norm_gain).astype(jnp.bfloat16)
    return (stream, normed)


def route_by_group(stream, normed, routes, route_weight, w_gate, w_up, w_down):
    shards = lax.axis_size("tp")
    seq_ranks = lax.axis_size("sp")
    block_rows, width = stream.shape
    local_experts = w_gate.shape[0]
    capacity = block_rows // seq_ranks
    group = routes[:, 0] // local_experts
    order = jnp.arange(block_rows, dtype=jnp.int32)
    earlier = (group[:, None] == group[None, :]) & (order[None, :] < order[:, None])
    slot = group * capacity + jnp.sum(earlier.astype(jnp.int32), axis=1)
    select = (order[:, None] == slot[None, :]).astype(jnp.bfloat16)
    member = routes[:, :, None] % local_experts == jnp.arange(local_experts, dtype=jnp.int32)
    weight = jnp.sum(jnp.where(member, route_weight[:, :, None], 0.0), axis=1)
    high = lax.reduce_precision(weight, 8, 7)
    labels = jnp.concatenate([high, weight - high], axis=1).astype(jnp.bfloat16)
    labels = jnp.pad(labels, ((0, 0), (0, LANES - labels.shape[1])))
    rows = jnp.concatenate([normed, labels], axis=1)
    outgoing = jnp.dot(select, rows, preferred_element_type=jnp.float32).astype(jnp.bfloat16)
    outgoing = outgoing.reshape(seq_ranks, capacity, width + LANES)
    arrived = lax.all_to_all(outgoing, "sp", split_axis=0, concat_axis=0, tiled=True)
    blocks = {0: arrived.reshape(block_rows, width + LANES)}
    bits = [1 << b for b in range(shards.bit_length() - 1)]
    for bit in reversed(bits):
        blocks.update({k | bit: flipped(v, "tp", bit) for k, v in blocks.items()})
    down = w_down.reshape(local_experts * w_down.shape[1], width)
    parts = {}
    for k, block in blocks.items():
        features = block[:, :width]
        marks = block[:, width:].astype(jnp.float32)
        hidden = []
        for expert in range(local_experts):
            gate = jnp.dot(features, w_gate[expert], preferred_element_type=jnp.float32)
            upper = jnp.dot(features, w_up[expert], preferred_element_type=jnp.float32)
            scale = marks[:, expert] + marks[:, local_experts + expert]
            hidden.append((jax.nn.silu(gate) * upper * scale[:, None]).astype(jnp.bfloat16))
        hidden = jnp.concatenate(hidden, axis=1)
        parts[k] = jnp.dot(hidden, down, preferred_element_type=jnp.float32)
    for bit in bits:
        for k in [k for k in parts if k & bit]:
            parts[k ^ bit] += flipped(parts.pop(k).astype(jnp.bfloat16), "tp", bit).astype(
                jnp.float32
            )
    summed = parts[0].astype(jnp.bfloat16).reshape(seq_ranks, capacity, width)
    returned = lax.all_to_all(summed, "sp", split_axis=0, concat_axis=0, tiled=True)
    weighted = lax.dot_general(
        select,
        returned.reshape(block_rows, width),
        (((0,), (0,)), ((), ())),
        preferred_element_type=jnp.float32,
    )
    return (stream + weighted).astype(jnp.bfloat16)


def route_by_expert(stream, normed, routes, route_weight, w_gate, w_up, w_down):
    shards = lax.axis_size("tp")
    seq_ranks = lax.axis_size("sp")
    block_rows, width = stream.shape
    local_experts = w_gate.shape[0]
    experts = local_experts * seq_ranks
    capacity = 2 * block_rows // experts
    flat_routes = routes.reshape(-1)
    position = jnp.arange(flat_routes.shape[0], dtype=jnp.int32)
    earlier = (flat_routes[:, None] == flat_routes[None, :]) & (
        position[None, :] < position[:, None]
    )
    rank = jnp.sum(earlier.astype(jnp.int32), axis=1)
    slot = flat_routes * capacity + rank
    outgoing = (
        jnp.zeros((experts * capacity, width), jnp.bfloat16).at[slot].set(normed[position // 2])
    )
    outgoing = outgoing.reshape(seq_ranks, local_experts, capacity, width)
    spread = lax.all_gather(
        lax.all_to_all(outgoing, "sp", split_axis=0, concat_axis=0, tiled=True)[:, None],
        "tp",
        axis=1,
        tiled=True,
    )
    count = spread.shape[3]
    partials = []
    for expert in range(local_experts):
        rows = spread[:, :, expert].reshape(seq_ranks * shards * count, width)
        gate = jnp.dot(rows, w_gate[expert], preferred_element_type=jnp.float32)
        upper = jnp.dot(rows, w_up[expert], preferred_element_type=jnp.float32)
        hidden = (jax.nn.silu(gate) * upper).astype(jnp.bfloat16)
        part = jnp.dot(hidden, w_down[expert], preferred_element_type=jnp.float32).astype(
            jnp.bfloat16
        )
        partials.append(part.reshape(seq_ranks, shards, count, width))
    stacked = jnp.stack(partials, axis=2)
    summed = lax.psum_scatter(stacked, "tp", scatter_dimension=1, tiled=True).astype(jnp.float32)
    returned = lax.all_to_all(
        summed[:, 0].astype(jnp.bfloat16), "sp", split_axis=0, concat_axis=0, tiled=True
    )
    results = returned.reshape(experts * capacity, width)[slot]
    results = results.reshape(block_rows, 2, width).astype(jnp.float32)
    weighted = jnp.sum(route_weight[:, :, None] * results, axis=1)
    return (stream + weighted).astype(jnp.bfloat16)


def on_device(
    conv_input,
    pre_gate,
    post_gate,
    conv_taps,
    out_proj,
    residual_in,
    norm_gain,
    routes,
    route_weight,
    w_gate,
    w_up,
    w_down,
):
    shards = lax.axis_size("tp")
    mixed = mix(conv_input, pre_gate, post_gate, conv_taps)
    stream, normed = project(mixed, out_proj, residual_in, norm_gain)
    whole_groups = lax.axis_size("sp") == GROUPS and shards & shards - 1 == 0
    route = route_by_group if whole_groups else route_by_expert
    return route(stream, normed, routes, route_weight, w_gate, w_up, w_down)


def solution(mesh):
    return jax.shard_map(
        on_device,
        mesh=mesh,
        in_specs=(
            P(("grp", "sp"), "tp"),
            P(("grp", "sp"), "tp"),
            P(("grp", "sp"), "tp"),
            P(),
            P(),
            P(("grp", "sp", "tp"), None),
            P(),
            P(("grp", "sp", "tp"), None),
            P(("grp", "sp", "tp"), None),
            P("sp", None, "tp"),
            P("sp", None, "tp"),
            P("sp", "tp", None),
        ),
        out_specs=P(("grp", "sp", "tp"), None),
        check_vma=False,
    )
```

profile of v0, /device:TPU:0, one launch (start us, length us, event | category | flops | bytes accessed | tf_op | source)
XLA Modules:
  0.0 97.2 jit_solution(9595113881826151975)
XLA Ops:
  0.0 0.8 slice.127
  0.8 0.7 slice.128
  1.5 5.0 %collective-permute-start = (bf16[2,512]{1,0:T(2,128)(2,1)S(1)}, bf16[2,512]{1,0:T(2,128)(2,1)S(1)}, u32[]{:S(2)}, u32[]{:S(2)}) collective-permute-start(bf16[2,512]{1,0:T(2,128)(2,1)S(1)} %pad_maximum_fusion.1), channel_id=1, source_target_pairs={{0,4},{4,8},{8,12},{1,5},{5,9},{9,13},{2,6},{6,10},{10,14},{3,7},{... | collective-permute-start | bytes 6152 | tf_op jit(solution)/shard_map/ppermute | solution.py:13
  6.5 0.7 fusion.111
  7.2 0.7 and_select_fusion.2
  7.9 0.7 and_select_fusion
  8.6 1.1 %convert_multiply_fusion = f32[512,256]{1,0:T(8,128)S(1)} fusion(bf16[512,256]{1,0:T(8,128)(2,1)} %param.12, bf16[512,256]{1,0:T(8,128)(2,1)} %param.13), kind=kLoop, calls=%fused_computation.78 | loop fusion | flops 393216 | bytes 1048576 | tf_op jit(solution)/shard_map/mul | solution.py:29
  9.7 0.7 fusion.108
  10.6 0.9 fusion.119
  11.6 1.9 %fusion.62 = bf16[512,256]{1,0:T(8,128)(2,1)} fusion(f32[2,256]{1,0:T(2,128)S(1)} %convert_multiply_fusion.1, f32[512,256]{1,0:T(8,128)S(1)} %convert_multiply_fusion, bf16[512,256]{1,0:T(8,128)(2,1)} %param.14, f32[256]{0:T(256)S(1)} %bitcast.96, f32[256]{0:T(256)S(1)} %bitcast.95, f32[256]{0:T(256)S(1)} %bitcast.94), kind=kLoop, calls=%fused_computation.75 | loop fusion | flops 1310720 | bytes 1053696 | tf_op jit(solution)/shard_map/convert_element_type | solution.py:34
  13.5 3.4 %all-to-all-start = ((bf16[4,128,256]{2,1,0:T(8,128)(2,1)}), bf16[4,128,256]{2,1,0:T(8,128)(2,1)S(1)}, u32[]{:S(2)}, u32[]{:S(2)}) async-start(bf16[4,128,256]{2,1,0:T(8,128)(2,1)} %bitcast.3), calls=%async_computation | async-start | bytes 524288 | tf_op jit(solution)/shard_map/all_to_all | solution.py:38
  16.9 5.9 %all-to-all-done = bf16[4,128,256]{2,1,0:T(8,128)(2,1)S(1)} async-done(((bf16[4,128,256]{2,1,0:T(8,128)(2,1)}), bf16[4,128,256]{2,1,0:T(8,128)(2,1)S(1)}, u32[]{:S(2)}, u32[]{:S(2)}) %all-to-all-start) | async-done | bytes 262176 | tf_op jit(solution)/shard_map/all_to_all | solution.py:38
  23.0 3.0 %multiply_reduce_fusion = (f32[128]{0:T(128)S(1)}, f32[128,2048]{1,0:T(8,128)S(1)}) fusion(bf16[128,1024]{0,1:T(8,128)(2,1)S(1)} %bitcast.84, bf16[1024,2048]{1,0:T(8,128)(2,1)} %param.16, bf16[128,2048]{1,0:T(8,128)(2,1)S(1)} %copy-done.1), kind=kOutput, calls=%fused_computation.47 | convolution fusion | flops 537919360 | bytes 6029824 | tf_op jit(solution)/shard_map/dot_general | solution.py:39
  26.6 18.7 %all_to_all.29 = bf16[4,32,2176]{2,1,0:T(8,128)(2,1)S(1)} all-to-all(bf16[4,32,2176]{2,1,0:T(8,128)(2,1)S(1)} %bitcast.93), channel_id=1, replica_groups=mesh['grp'=2,'sp'=4,'tp'=4] {'sp'}, dimensions={0} | all-to-all | bytes 1114112 | tf_op jit(solution)/shard_map/all_to_all | solution.py:65
  45.3 0.8 collective-permute-start.3
  46.6 0.3 fusion.34
  47.0 0.3 fusion.4
  47.3 0.8 collective-permute-done.1
  48.2 0.3 fusion.17
  49.6 0.4 convolution_convert_fusion.2
  50.0 8.4 %collective-permute-done.3 = bf16[128,2176]{1,0:T(8,128)(2,1)S(1)} collective-permute-done((bf16[128,2176]{1,0:T(8,128)(2,1)S(1)}, bf16[128,2176]{1,0:T(8,128)(2,1)S(1)}, u32[]{:S(2)}, u32[]{:S(2)}) %collective-permute-start.3) | collective-permute-done | bytes 557088 | tf_op jit(solution)/shard_map/ppermute | solution.py:17
  58.6 0.6 collective-permute-start.2
  59.9 0.5 collective-permute-done.4
  61.3 0.3 multiply_convert_fusion.1
  61.9 0.4 convolution_convert_fusion.1
  63.2 1.1 %collective-permute-done.5 = bf16[128,2048]{1,0:T(8,128)(2,1)S(1)} collective-permute-done((bf16[128,2048]{1,0:T(8,128)(2,1)S(1)}, bf16[128,2048]{1,0:T(8,128)(2,1)S(1)}, u32[]{:S(2)}, u32[]{:S(2)}) %collective-permute-start.5) | collective-permute-done | bytes 524320 | tf_op jit(solution)/shard_map/ppermute | solution.py:17
  64.3 0.4 add_convert_fusion.1
  64.8 1.4 %collective-permute-start.6 = (bf16[128,2048]{1,0:T(8,128)(2,1)S(1)}, bf16[128,2048]{1,0:T(8,128)(2,1)S(1)}, u32[]{:S(2)}, u32[]{:S(2)}) collective-permute-start(bf16[128,2048]{1,0:T(8,128)(2,1)S(1)} %add_convert_fusion.1), channel_id=1, source_target_pairs={{0,2},{1,3},{2,0},{3,1},{4,6},{5,7},{6,4},{7,5},{8,10},{9,11},{10,... | collective-permute-start | bytes 1572872 | tf_op jit(solution)/shard_map/ppermute | solution.py:17
  66.5 0.4 fusion.81
  67.0 11.9 %collective-permute-done.6 = bf16[128,2048]{1,0:T(8,128)(2,1)S(1)} collective-permute-done((bf16[128,2048]{1,0:T(8,128)(2,1)S(1)}, bf16[128,2048]{1,0:T(8,128)(2,1)S(1)}, u32[]{:S(2)}, u32[]{:S(2)}) %collective-permute-start.6) | collective-permute-done | bytes 524320 | tf_op jit(solution)/shard_map/ppermute | solution.py:17
  79.0 17.0 %all_to_all.30 = bf16[4,32,2048]{2,1,0:T(8,128)(2,1)S(1)} all-to-all(bf16[4,32,2048]{2,1,0:T(8,128)(2,1)S(1)} %bitcast.82), channel_id=1, replica_groups=mesh['grp'=2,'sp'=4,'tp'=4] {'sp'}, dimensions={0} | all-to-all | bytes 1048576 | tf_op jit(solution)/shard_map/all_to_all | solution.py:89
  96.1 1.1 %fusion = bf16[128,2048]{1,0:T(8,128)(2,1)} fusion(f32[128,2048]{1,0:T(8,128)S(1)} %get-tuple-element.19, bf16[128,2048]{1,0:T(8,128)(2,1)S(1)} %bitcast.83, s32[128]{0:T(128)S(1)} %multiply_add_fusion), kind=kOutput, calls=%fused_computation.3 | convolution fusion | flops 67649536 | bytes 2097664 | tf_op jit(solution)/shard_map/dot_general | solution.py:90
  (49 shorter events, 6.1 us)
Async XLA Ops:
  0.0 49.6 %copy-start = (bf16[2,256,2048]{2,1,0:T(8,128)(2,1)S(1)}, bf16[2,256,2048]{2,1,0:T(8,128)(2,1)}, u32[]{:S(2)}) copy-start(bf16[2,256,2048]{2,1,0:T(8,128)(2,1)} %param.23) | copy-start | bytes 6291460
  0.0 16.9 %copy-start.3 = (s32[128,2]{0,1:T(2,128)S(1)}, s32[128,2]{0,1:T(2,128)}, u32[]{:S(2)}) copy-start(s32[128,2]{0,1:T(2,128)} %param.19) | copy-start | bytes 3076
  0.0 23.0 %copy-start.1 = (bf16[128,2048]{1,0:T(8,128)(2,1)S(1)}, bf16[128,2048]{1,0:T(8,128)(2,1)}, u32[]{:S(2)}) copy-start(bf16[128,2048]{1,0:T(8,128)(2,1)} %param.17) | copy-start | bytes 1572868
  1.5 10.0 %collective-permute-start = (bf16[2,512]{1,0:T(2,128)(2,1)S(1)}, bf16[2,512]{1,0:T(2,128)(2,1)S(1)}, u32[]{:S(2)}, u32[]{:S(2)}) collective-permute-start(bf16[2,512]{1,0:T(2,128)(2,1)S(1)} %pad_maximum_fusion.1), channel_id=1, source_target_pairs={{0,4},{4,8},{8,12},{1,5},{5,9},{9,13},{2,6},{6,10},{10,14},{3,7},{... | collective-permute-start | bytes 6152 | tf_op jit(solution)/shard_map/ppermute | solution.py:13
  13.5 9.4 %all-to-all-start = ((bf16[4,128,256]{2,1,0:T(8,128)(2,1)}), bf16[4,128,256]{2,1,0:T(8,128)(2,1)S(1)}, u32[]{:S(2)}, u32[]{:S(2)}) async-start(bf16[4,128,256]{2,1,0:T(8,128)(2,1)} %bitcast.3), calls=%async_computation | async-start | bytes 524288 | tf_op jit(solution)/shard_map/all_to_all | solution.py:38
  23.0 3.0 %copy-start.2 = (f32[2048]{0:T(1024)S(1)}, f32[2048]{0:T(1024)}, u32[]{:S(2)}) copy-start(f32[2048]{0:T(1024)} %param.18) | copy-start | bytes 24580
  26.1 20.0 %copy-start.4 = (bf16[2,2048,256]{2,1,0:T(8,128)(2,1)S(1)}, bf16[2,2048,256]{2,1,0:T(8,128)(2,1)}, u32[]{:S(2)}) copy-start(bf16[2,2048,256]{2,1,0:T(8,128)(2,1)} %param.21) | copy-start | bytes 6291460
  45.3 1.7 %copy-start.5 = (bf16[2,2048,256]{2,1,0:T(8,128)(2,1)S(1)}, bf16[2,2048,256]{2,1,0:T(8,128)(2,1)}, u32[]{:S(2)}) copy-start(bf16[2,2048,256]{2,1,0:T(8,128)(2,1)} %param.22) | copy-start | bytes 6291460
  45.3 13.2 %collective-permute-start.3 = (bf16[128,2176]{1,0:T(8,128)(2,1)S(1)}, bf16[128,2176]{1,0:T(8,128)(2,1)S(1)}, u32[]{:S(2)}, u32[]{:S(2)}) collective-permute-start(bf16[128,2176]{1,0:T(8,128)(2,1)S(1)} %bitcast.87), channel_id=1, source_target_pairs={{0,2},{1,3},{2,0},{3,1},{4,6},{5,7},{6,4},{7,5},{8,10},{9,11},{10,... | collective-permute-start | bytes 1671176 | tf_op jit(solution)/shard_map/ppermute | solution.py:17
  46.1 2.0 %collective-permute-start.1 = (bf16[128,2176]{1,0:T(8,128)(2,1)S(1)}, bf16[128,2176]{1,0:T(8,128)(2,1)S(1)}, u32[]{:S(2)}, u32[]{:S(2)}) collective-permute-start(bf16[128,2176]{1,0:T(8,128)(2,1)S(1)} %bitcast.88), channel_id=1, source_target_pairs={{0,1},{1,0},{2,3},{3,2},{4,5},{5,4},{6,7},{7,6},{8,9},{9,8},{10,11... | collective-permute-start | bytes 1671176 | tf_op jit(solution)/shard_map/ppermute | solution.py:17
  58.4 2.0 %collective-permute-start.4 = (bf16[128,2176]{1,0:T(8,128)(2,1)S(1)}, bf16[128,2176]{1,0:T(8,128)(2,1)S(1)}, u32[]{:S(2)}, u32[]{:S(2)}) collective-permute-start(bf16[128,2176]{1,0:T(8,128)(2,1)S(1)} %collective-permute-done.3), channel_id=1, source_target_pairs={{0,1},{1,0},{2,3},{3,2},{4,5},{5,4},{6,7},{7,6},{8,9},{9,8},{10,11... | collective-permute-start | bytes 1671176 | tf_op jit(solution)/shard_map/ppermute | solution.py:17
  58.6 8.3 %collective-permute-start.2 = (bf16[128,2048]{1,0:T(8,128)(2,1)S(1)}, bf16[128,2048]{1,0:T(8,128)(2,1)S(1)}, u32[]{:S(2)}, u32[]{:S(2)}) collective-permute-start(bf16[128,2048]{1,0:T(8,128)(2,1)S(1)} %convolution_convert_fusion.2), channel_id=1, source_target_pairs={{0,1},{1,0},{2,3},{3,2},{4,5},{5,4},{6,7},{7,6},{8,9},{9,8},{10,11... | collective-permute-start | bytes 1572872 | tf_op jit(solution)/shard_map/ppermute | solution.py:17
  62.4 2.0 %collective-permute-start.5 = (bf16[128,2048]{1,0:T(8,128)(2,1)S(1)}, bf16[128,2048]{1,0:T(8,128)(2,1)S(1)}, u32[]{:S(2)}, u32[]{:S(2)}) collective-permute-start(bf16[128,2048]{1,0:T(8,128)(2,1)S(1)} %convolution_convert_fusion.1), channel_id=1, source_target_pairs={{0,1},{1,0},{2,3},{3,2},{4,5},{5,4},{6,7},{7,6},{8,9},{9,8},{10,11... | collective-permute-start | bytes 1572872 | tf_op jit(solution)/shard_map/ppermute | solution.py:17
  64.8 14.0 %collective-permute-start.6 = (bf16[128,2048]{1,0:T(8,128)(2,1)S(1)}, bf16[128,2048]{1,0:T(8,128)(2,1)S(1)}, u32[]{:S(2)}, u32[]{:S(2)}) collective-permute-start(bf16[128,2048]{1,0:T(8,128)(2,1)S(1)} %add_convert_fusion.1), channel_id=1, source_target_pairs={{0,2},{1,3},{2,0},{3,1},{4,6},{5,7},{6,4},{7,5},{8,10},{9,11},{10,... | collective-permute-start | bytes 1572872 | tf_op jit(solution)/shard_map/ppermute | solution.py:17
where the time goes:
time: 97.7 us; the launch traced here: 97.2 us
  blocking collectives  35.7 us (37%)
  waiting for transfers between devices  28.6 us (29%)
  matrix products  11.4 us (12%)
  starting transfers between devices  11.3 us (12%)
  other arithmetic  7.07 us (7%)
  local copies, waits for them, and re-layouts  2.75 us (3%)
    ppermute x6, waiting for transfers between devices, flipped(): lax.ppermute(block, axis, [(i, i ^ bit) for i in range(lax.axis_size(axis...  22.7 us
    all_to_all x1, blocking collectives, route_by_group(): lax.all_to_all(outgoing, 'sp', split_axis=0, concat_axis=0, tiled=True)  18.7 us
    all_to_all x1, blocking collectives, route_by_group(): lax.all_to_all(summed, 'sp', split_axis=0, concat_axis=0, tiled=True)  17 us
    all_to_all x1, waiting for transfers between devices, project(): lax.all_to_all(mixed, 'tp', split_axis=0, concat_axis=1, tiled=True)  5.94 us
    ppermute x1, starting transfers between devices, shifted(): return lax.ppermute(block, axis, route)  4.96 us
    all_to_all x1, starting transfers between devices, project(): lax.all_to_all(mixed, 'tp', split_axis=0, concat_axis=1, tiled=True)  3.41 us
    dot_general x1, matrix products, project(): jnp.dot(token_rows, out_proj, preferred_element_type=jnp.float32)  3.01 us
    ppermute x6, starting transfers between devices, flipped(): lax.ppermute(block, axis, [(i, i ^ bit) for i in range(lax.axis_size(axis...  2.97 us
  transfers between devices with their start and end apart: 8, of which 6 were waited for; matrix products, arithmetic and copies ran while one was open for 13% of the time, Pallas kernels for 0%

commit v1 on v0

--- a/solution.py
+++ b/solution.py
@@ -5,6 +5,22 @@
 
 GROUPS = 4
 LANES = 128
+
+
+def swapped_with_each(x, axis, split, join):
+    ways, here = (lax.axis_size(axis), lax.axis_index(axis))
+    width = x.shape[split] // ways
+    dims = list(x.shape)
+    dims[split] = width
+    height = dims[join]
+    dims[join] = height * ways
+    full = jnp.zeros(dims, x.dtype)
+    for mask in range(ways):
+        part = lax.dynamic_slice_in_dim(x, (here ^ mask) * width, width, axis=split)
+        if mask:
+            part = lax.ppermute(part, axis, [(d, d ^ mask) for d in range(ways)])
+        full = lax.dynamic_update_slice_in_dim(full, part, (here ^ mask) * height, axis=join)
+    return full
 
 
 def shifted(block, axis, distance):
@@ -62,7 +78,7 @@
     rows = jnp.concatenate([normed, labels], axis=1)
     outgoing = jnp.dot(select, rows, preferred_element_type=jnp.float32).astype(jnp.bfloat16)
     outgoing = outgoing.reshape(seq_ranks, capacity, width + LANES)
-    arrived = lax.all_to_all(outgoing, "sp", split_axis=0, concat_axis=0, tiled=True)
+    arrived = swapped_with_each(outgoing, "sp", 0, 0)
     blocks = {0: arrived.reshape(block_rows, width + LANES)}
     bits = [1 << b for b in range(shards.bit_length() - 1)]
     for bit in reversed(bits):

time: 97.7 us -> 95.6 us (0.979)
  blocking collectives: 35.7 us -> 16.9 us
  waiting for transfers between devices: 28.6 us -> 42 us
  starting transfers between devices: 11.3 us -> 14.3 us
    all_to_all x1 -> x0, blocking collectives: 18.7 us -> none  [route_by_group(): lax.all_to_all(outgoing, 'sp', split_axis=0, concat_axis=0, tiled=True)]
    ppermute x0 -> x3, waiting for transfers between devices: none -> 11.4 us  [swapped_with_each(): part = lax.ppermute(part, axis, [(d, d ^ mask) for d in range(ways)])]
    ppermute x0 -> x3, starting transfers between devices: none -> 4.12 us  [swapped_with_each(): part = lax.ppermute(part, axis, [(d, d ^ mask) for d in range(ways)])]
    ppermute x6, waiting for transfers between devices: 22.7 us -> 24.7 us  [flipped(): lax.ppermute(block, axis, [(i, i ^ bit) for i in range(lax.axis_size(axis...]
    ppermute x6, starting transfers between devices: 2.97 us -> 1.79 us  [flipped(): lax.ppermute(block, axis, [(i, i ^ bit) for i in range(lax.axis_size(axis...]
  transfers between devices with their start and end apart: 8 -> 11, of which waited for: 6 -> 8; matrix products, arithmetic and copies ran while one was open for 13% -> 13% of each run, Pallas kernels for 0% -> 0%
where the time goes in v1:
time: 95.6 us; the launch traced here: 95.1 us
  waiting for transfers between devices  42 us (44%)
  blocking collectives  16.9 us (18%)
  starting transfers between devices  14.3 us (15%)
  matrix products  11.4 us (12%)
  other arithmetic  7.08 us (7%)
  local copies, waits for them, and re-layouts  3.01 us (3%)
    ppermute x6, waiting for transfers between devices, flipped(): lax.ppermute(block, axis, [(i, i ^ bit) for i in range(lax.axis_size(axis...  24.7 us
    all_to_all x1, blocking collectives, route_by_group(): lax.all_to_all(summed, 'sp', split_axis=0, concat_axis=0, tiled=True)  16.9 us
    ppermute x3, waiting for transfers between devices, swapped_with_each(): part = lax.ppermute(part, axis, [(d, d ^ mask) for d in range(ways)])  11.4 us
    all_to_all x1, waiting for transfers between devices, project(): lax.all_to_all(mixed, 'tp', split_axis=0, concat_axis=1, tiled=True)  5.94 us
    ppermute x1, starting transfers between devices, shifted(): return lax.ppermute(block, axis, route)  4.96 us
    ppermute x3, starting transfers between devices, swapped_with_each(): part = lax.ppermute(part, axis, [(d, d ^ mask) for d in range(ways)])  4.12 us
    all_to_all x1, starting transfers between devices, project(): lax.all_to_all(mixed, 'tp', split_axis=0, concat_axis=1, tiled=True)  3.41 us
    dot_general x1, matrix products, project(): jnp.dot(token_rows, out_proj, preferred_element_type=jnp.float32)  3.01 us
  transfers between devices with their start and end apart: 11, of which 8 were waited for; matrix products, arithmetic and copies ran while one was open for 13% of the time, Pallas kernels for 0%

profile of v1, /device:TPU:0, one launch (start us, length us, event | category | flops | bytes accessed | tf_op | source)
XLA Modules:
  0.0 95.1 jit_solution(12640609238236185002)
XLA Ops:
  0.0 0.8 slice.127
  0.8 0.7 slice.128
  1.5 5.0 %collective-permute-start = (bf16[2,512]{1,0:T(2,128)(2,1)S(1)}, bf16[2,512]{1,0:T(2,128)(2,1)S(1)}, u32[]{:S(2)}, u32[]{:S(2)}) collective-permute-start(bf16[2,512]{1,0:T(2,128)(2,1)S(1)} %pad_maximum_fusion.1), channel_id=1, source_target_pairs={{0,4},{4,8},{8,12},{1,5},{5,9},{9,13},{2,6},{6,10},{10,14},{3,7},{... | collective-permute-start | bytes 6152 | tf_op jit(solution)/shard_map/ppermute | solution.py:29
  6.5 0.7 fusion.109
  7.2 0.7 and_select_fusion.2
  7.9 0.7 and_select_fusion
  8.6 1.1 %convert_multiply_fusion = f32[512,256]{1,0:T(8,128)S(1)} fusion(bf16[512,256]{1,0:T(8,128)(2,1)} %param.12, bf16[512,256]{1,0:T(8,128)(2,1)} %param.13), kind=kLoop, calls=%fused_computation.74 | loop fusion | flops 393216 | bytes 1048576 | tf_op jit(solution)/shard_map/mul | solution.py:45
  9.7 0.7 fusion.106
  10.6 0.9 fusion.117
  11.6 1.9 %fusion.60 = bf16[512,256]{1,0:T(8,128)(2,1)} fusion(f32[2,256]{1,0:T(2,128)S(1)} %convert_multiply_fusion.1, f32[512,256]{1,0:T(8,128)S(1)} %convert_multiply_fusion, bf16[512,256]{1,0:T(8,128)(2,1)} %param.14, f32[256]{0:T(256)S(1)} %bitcast.100, f32[256]{0:T(256)S(1)} %bitcast.99, f32[256]{0:T(256)S(1)} %bitcast.98), kind=kLoop, calls=%fused_computation.71 | loop fusion | flops 1310720 | bytes 1053696 | tf_op jit(solution)/shard_map/convert_element_type | solution.py:50
  13.5 3.4 %all-to-all-start = ((bf16[4,128,256]{2,1,0:T(8,128)(2,1)}), bf16[4,128,256]{2,1,0:T(8,128)(2,1)S(1)}, u32[]{:S(2)}, u32[]{:S(2)}) async-start(bf16[4,128,256]{2,1,0:T(8,128)(2,1)} %bitcast.3), calls=%async_computation | async-start | bytes 524288 | tf_op jit(solution)/shard_map/all_to_all | solution.py:54
  16.9 5.9 %all-to-all-done = bf16[4,128,256]{2,1,0:T(8,128)(2,1)S(1)} async-done(((bf16[4,128,256]{2,1,0:T(8,128)(2,1)}), bf16[4,128,256]{2,1,0:T(8,128)(2,1)S(1)}, u32[]{:S(2)}, u32[]{:S(2)}) %all-to-all-start) | async-done | bytes 262176 | tf_op jit(solution)/shard_map/all_to_all | solution.py:54
  23.1 3.0 %multiply_reduce_fusion = (f32[128]{0:T(128)S(1)}, f32[128,2048]{1,0:T(8,128)S(1)}) fusion(bf16[128,1024]{0,1:T(8,128)(2,1)S(1)} %bitcast.88, bf16[1024,2048]{1,0:T(8,128)(2,1)} %param.16, bf16[128,2048]{1,0:T(8,128)(2,1)S(1)} %copy-done.1), kind=kOutput, calls=%fused_computation.43 | convolution fusion | flops 537919360 | bytes 6029824 | tf_op jit(solution)/shard_map/dot_general | solution.py:55
  26.7 1.6 %collective-permute-start.1 = (bf16[1,32,2176]{2,1,0:T(8,128)(2,1)S(1)}, bf16[1,32,2176]{2,1,0:T(8,128)(2,1)S(1)}, u32[]{:S(2)}, u32[]{:S(2)}) collective-permute-start(bf16[1,32,2176]{2,1,0:T(8,128)(2,1)S(1)} %get-tuple-element.15), channel_id=1, source_target_pairs={{0,4},{4,0},{8,12},{12,8},{1,5},{5,1},{9,13},{13,9},{2,6},{6,2},{1... | collective-permute-start | bytes 417800 | tf_op jit(solution)/shard_map/ppermute | solution.py:21
  28.3 2.5 %collective-permute-start.3 = (bf16[1,32,2176]{2,1,0:T(8,128)(2,1)S(1)}, bf16[1,32,2176]{2,1,0:T(8,128)(2,1)S(1)}, u32[]{:S(2)}, u32[]{:S(2)}) collective-permute-start(bf16[1,32,2176]{2,1,0:T(8,128)(2,1)S(1)} %get-tuple-element.13), channel_id=1, source_target_pairs={{0,12},{4,8},{8,4},{12,0},{1,13},{5,9},{9,5},{13,1},{2,14},{6,10},... | collective-permute-start | bytes 417800 | tf_op jit(solution)/shard_map/ppermute | solution.py:21
  30.8 1.1 %collective-permute-done.1 = bf16[1,32,2176]{2,1,0:T(8,128)(2,1)S(1)} collective-permute-done((bf16[1,32,2176]{2,1,0:T(8,128)(2,1)S(1)}, bf16[1,32,2176]{2,1,0:T(8,128)(2,1)S(1)}, u32[]{:S(2)}, u32[]{:S(2)}) %collective-permute-start.1) | collective-permute-done | bytes 139296 | tf_op jit(solution)/shard_map/ppermute | solution.py:21
  31.9 10.3 %collective-permute-done.2 = bf16[1,32,2176]{2,1,0:T(8,128)(2,1)S(1)} collective-permute-done((bf16[1,32,2176]{2,1,0:T(8,128)(2,1)S(1)}, bf16[1,32,2176]{2,1,0:T(8,128)(2,1)S(1)}, u32[]{:S(2)}, u32[]{:S(2)}) %collective-permute-start.2) | collective-permute-done | bytes 139296 | tf_op jit(solution)/shard_map/ppermute | solution.py:21
  42.3 0.6 collective-permute-start.6
  43.5 0.3 fusion.32
  44.2 0.7 collective-permute-done.4
  46.4 0.4 convolution_convert_fusion.2
  46.9 9.6 %collective-permute-done.6 = bf16[128,2176]{1,0:T(8,128)(2,1)S(1)} collective-permute-done((bf16[128,2176]{1,0:T(8,128)(2,1)S(1)}, bf16[128,2176]{1,0:T(8,128)(2,1)S(1)}, u32[]{:S(2)}, u32[]{:S(2)}) %collective-permute-start.6) | collective-permute-done | bytes 557088 | tf_op jit(solution)/shard_map/ppermute | solution.py:33
  56.6 0.6 collective-permute-start.5
  57.9 0.5 collective-permute-done.7
  59.9 0.4 convolution_convert_fusion.1
  61.2 1.1 %collective-permute-done.8 = bf16[128,2048]{1,0:T(8,128)(2,1)S(1)} collective-permute-done((bf16[128,2048]{1,0:T(8,128)(2,1)S(1)}, bf16[128,2048]{1,0:T(8,128)(2,1)S(1)}, u32[]{:S(2)}, u32[]{:S(2)}) %collective-permute-start.8) | collective-permute-done | bytes 524320 | tf_op jit(solution)/shard_map/ppermute | solution.py:33
  62.4 0.4 add_convert_fusion.1
  62.8 0.4 collective-permute-start.9
  63.5 0.4 fusion.79
  64.0 12.8 %collective-permute-done.9 = bf16[128,2048]{1,0:T(8,128)(2,1)S(1)} collective-permute-done((bf16[128,2048]{1,0:T(8,128)(2,1)S(1)}, bf16[128,2048]{1,0:T(8,128)(2,1)S(1)}, u32[]{:S(2)}, u32[]{:S(2)}) %collective-permute-start.9) | collective-permute-done | bytes 524320 | tf_op jit(solution)/shard_map/ppermute | solution.py:33
  77.1 16.9 %all_to_all.24 = bf16[4,32,2048]{2,1,0:T(8,128)(2,1)S(1)} all-to-all(bf16[4,32,2048]{2,1,0:T(8,128)(2,1)S(1)} %bitcast.86), channel_id=1, replica_groups=mesh['grp'=2,'sp'=4,'tp'=4] {'sp'}, dimensions={0} | all-to-all | bytes 1048576 | tf_op jit(solution)/shard_map/all_to_all | solution.py:105
  93.9 1.1 %fusion = bf16[128,2048]{1,0:T(8,128)(2,1)} fusion(f32[128,2048]{1,0:T(8,128)S(1)} %get-tuple-element.23, bf16[128,2048]{1,0:T(8,128)(2,1)S(1)} %bitcast.87, s32[128]{0:T(128)S(1)} %multiply_add_fusion), kind=kOutput, calls=%fused_computation.3 | convolution fusion | flops 67649536 | bytes 2097664 | tf_op jit(solution)/shard_map/dot_general | solution.py:106
  (59 shorter events, 7.3 us)
Async XLA Ops:
  0.0 46.4 %copy-start = (bf16[2,256,2048]{2,1,0:T(8,128)(2,1)S(1)}, bf16[2,256,2048]{2,1,0:T(8,128)(2,1)}, u32[]{:S(2)}) copy-start(bf16[2,256,2048]{2,1,0:T(8,128)(2,1)} %param.23) | copy-start | bytes 6291460
  0.0 16.9 %copy-start.3 = (s32[128,2]{0,1:T(2,128)S(1)}, s32[128,2]{0,1:T(2,128)}, u32[]{:S(2)}) copy-start(s32[128,2]{0,1:T(2,128)} %param.19) | copy-start | bytes 3076
  0.0 23.0 %copy-start.1 = (bf16[128,2048]{1,0:T(8,128)(2,1)S(1)}, bf16[128,2048]{1,0:T(8,128)(2,1)}, u32[]{:S(2)}) copy-start(bf16[128,2048]{1,0:T(8,128)(2,1)} %param.17) | copy-start | bytes 1572868
  1.5 10.1 %collective-permute-start = (bf16[2,512]{1,0:T(2,128)(2,1)S(1)}, bf16[2,512]{1,0:T(2,128)(2,1)S(1)}, u32[]{:S(2)}, u32[]{:S(2)}) collective-permute-start(bf16[2,512]{1,0:T(2,128)(2,1)S(1)} %pad_maximum_fusion.1), channel_id=1, source_target_pairs={{0,4},{4,8},{8,12},{1,5},{5,9},{9,13},{2,6},{6,10},{10,14},{3,7},{... | collective-permute-start | bytes 6152 | tf_op jit(solution)/shard_map/ppermute | solution.py:29
  13.5 9.4 %all-to-all-start = ((bf16[4,128,256]{2,1,0:T(8,128)(2,1)}), bf16[4,128,256]{2,1,0:T(8,128)(2,1)S(1)}, u32[]{:S(2)}, u32[]{:S(2)}) async-start(bf16[4,128,256]{2,1,0:T(8,128)(2,1)} %bitcast.3), calls=%async_computation | async-start | bytes 524288 | tf_op jit(solution)/shard_map/all_to_all | solution.py:54
  23.1 3.0 %copy-start.2 = (f32[2048]{0:T(1024)S(1)}, f32[2048]{0:T(1024)}, u32[]{:S(2)}) copy-start(f32[2048]{0:T(1024)} %param.18) | copy-start | bytes 24580
  26.3 16.7 %copy-start.4 = (bf16[2,2048,256]{2,1,0:T(8,128)(2,1)S(1)}, bf16[2,2048,256]{2,1,0:T(8,128)(2,1)}, u32[]{:S(2)}) copy-start(bf16[2,2048,256]{2,1,0:T(8,128)(2,1)} %param.21) | copy-start | bytes 6291460
  26.7 5.2 %collective-permute-start.1 = (bf16[1,32,2176]{2,1,0:T(8,128)(2,1)S(1)}, bf16[1,32,2176]{2,1,0:T(8,128)(2,1)S(1)}, u32[]{:S(2)}, u32[]{:S(2)}) collective-permute-start(bf16[1,32,2176]{2,1,0:T(8,128)(2,1)S(1)} %get-tuple-element.15), channel_id=1, source_target_pairs={{0,4},{4,0},{8,12},{12,8},{1,5},{5,1},{9,13},{13,9},{2,6},{6,2},{1... | collective-permute-start | bytes 417800 | tf_op jit(solution)/shard_map/ppermute | solution.py:21
  28.3 13.9 %collective-permute-start.3 = (bf16[1,32,2176]{2,1,0:T(8,128)(2,1)S(1)}, bf16[1,32,2176]{2,1,0:T(8,128)(2,1)S(1)}, u32[]{:S(2)}, u32[]{:S(2)}) collective-permute-start(bf16[1,32,2176]{2,1,0:T(8,128)(2,1)S(1)} %get-tuple-element.13), channel_id=1, source_target_pairs={{0,12},{4,8},{8,4},{12,0},{1,13},{5,9},{9,5},{13,1},{2,14},{6,10},... | collective-permute-start | bytes 417800 | tf_op jit(solution)/shard_map/ppermute | solution.py:21
  30.8 11.4 %collective-permute-start.2 = (bf16[1,32,2176]{2,1,0:T(8,128)(2,1)S(1)}, bf16[1,32,2176]{2,1,0:T(8,128)(2,1)S(1)}, u32[]{:S(2)}, u32[]{:S(2)}) collective-permute-start(bf16[1,32,2176]{2,1,0:T(8,128)(2,1)S(1)} %get-tuple-element.14), channel_id=1, source_target_pairs={{0,8},{4,12},{8,0},{12,4},{1,9},{5,13},{9,1},{13,5},{2,10},{6,14},... | collective-permute-start | bytes 417800 | tf_op jit(solution)/shard_map/ppermute | solution.py:21
  42.3 1.6 %copy-start.5 = (bf16[2,2048,256]{2,1,0:T(8,128)(2,1)S(1)}, bf16[2,2048,256]{2,1,0:T(8,128)(2,1)}, u32[]{:S(2)}) copy-start(bf16[2,2048,256]{2,1,0:T(8,128)(2,1)} %param.22) | copy-start | bytes 6291460
  42.3 14.1 %collective-permute-start.6 = (bf16[128,2176]{1,0:T(8,128)(2,1)S(1)}, bf16[128,2176]{1,0:T(8,128)(2,1)S(1)}, u32[]{:S(2)}, u32[]{:S(2)}) collective-permute-start(bf16[128,2176]{1,0:T(8,128)(2,1)S(1)} %bitcast.91), channel_id=1, source_target_pairs={{0,2},{1,3},{2,0},{3,1},{4,6},{5,7},{6,4},{7,5},{8,10},{9,11},{10,... | collective-permute-start | bytes 1671176 | tf_op jit(solution)/shard_map/ppermute | solution.py:33
  42.9 2.0 %collective-permute-start.4 = (bf16[128,2176]{1,0:T(8,128)(2,1)S(1)}, bf16[128,2176]{1,0:T(8,128)(2,1)S(1)}, u32[]{:S(2)}, u32[]{:S(2)}) collective-permute-start(bf16[128,2176]{1,0:T(8,128)(2,1)S(1)} %bitcast.92), channel_id=1, source_target_pairs={{0,1},{1,0},{2,3},{3,2},{4,5},{5,4},{6,7},{7,6},{8,9},{9,8},{10,11... | collective-permute-start | bytes 1671176 | tf_op jit(solution)/shard_map/ppermute | solution.py:33
  56.4 2.0 %collective-permute-start.7 = (bf16[128,2176]{1,0:T(8,128)(2,1)S(1)}, bf16[128,2176]{1,0:T(8,128)(2,1)S(1)}, u32[]{:S(2)}, u32[]{:S(2)}) collective-permute-start(bf16[128,2176]{1,0:T(8,128)(2,1)S(1)} %collective-permute-done.6), channel_id=1, source_target_pairs={{0,1},{1,0},{2,3},{3,2},{4,5},{5,4},{6,7},{7,6},{8,9},{9,8},{10,11... | collective-permute-start | bytes 1671176 | tf_op jit(solution)/shard_map/ppermute | solution.py:33
  56.6 7.3 %collective-permute-start.5 = (bf16[128,2048]{1,0:T(8,128)(2,1)S(1)}, bf16[128,2048]{1,0:T(8,128)(2,1)S(1)}, u32[]{:S(2)}, u32[]{:S(2)}) collective-permute-start(bf16[128,2048]{1,0:T(8,128)(2,1)S(1)} %convolution_convert_fusion.2), channel_id=1, source_target_pairs={{0,1},{1,0},{2,3},{3,2},{4,5},{5,4},{6,7},{7,6},{8,9},{9,8},{10,11... | collective-permute-start | bytes 1572872 | tf_op jit(solution)/shard_map/ppermute | solution.py:33
  60.4 2.0 %collective-permute-start.8 = (bf16[128,2048]{1,0:T(8,128)(2,1)S(1)}, bf16[128,2048]{1,0:T(8,128)(2,1)S(1)}, u32[]{:S(2)}, u32[]{:S(2)}) collective-permute-start(bf16[128,2048]{1,0:T(8,128)(2,1)S(1)} %convolution_convert_fusion.1), channel_id=1, source_target_pairs={{0,1},{1,0},{2,3},{3,2},{4,5},{5,4},{6,7},{7,6},{8,9},{9,8},{10,11... | collective-permute-start | bytes 1572872 | tf_op jit(solution)/shard_map/ppermute | solution.py:33
  62.8 14.0 %collective-permute-start.9 = (bf16[128,2048]{1,0:T(8,128)(2,1)S(1)}, bf16[128,2048]{1,0:T(8,128)(2,1)S(1)}, u32[]{:S(2)}, u32[]{:S(2)}) collective-permute-start(bf16[128,2048]{1,0:T(8,128)(2,1)S(1)} %add_convert_fusion.1), channel_id=1, source_target_pairs={{0,2},{1,3},{2,0},{3,1},{4,6},{5,7},{6,4},{7,5},{8,10},{9,11},{10,... | collective-permute-start | bytes 1572872 | tf_op jit(solution)/shard_map/ppermute | solution.py:33
